TPU v7x, 32 devices: a whole 2x2x4 slice. The times are simulated.
32 devices in a mesh: grp: 2 (over x), sp: 4 (over y, core), tp: 4 (over z).
Axes of the slice: x: 2, y: 2, z: 4, core: 2. Of those that a mesh axis runs over, the one named last changes fastest.
Arguments:
- layer_input: bfloat16 [8, 1024, 2048], P(('grp', 'tp'), 'sp'), parts along dimension 0, may hold values from -6 to 6
- norm_gain: bfloat16 [2048], replicated, may hold values from 0.099609375 to 1.8984375
- key_weight: bfloat16 [2048, 1024], replicated, may hold values from -0.125 to 0.125
- value_weight: bfloat16 [2048, 1024], replicated, may hold values from -0.125 to 0.125
- input_gate_weight: bfloat16 [2048, 8], replicated, may hold values from -0.125 to 0.125
- forget_gate_weight: bfloat16 [2048, 8], replicated, may hold values from -0.125 to 0.125
- conv_weight: float32 [4, 1024], replicated, may hold values from -3 to 3
- input_shift: float32 [8, 8, 1024], P(('grp', 'sp'), 'tp'), parts along dimension 0, may hold values from -4 to 302
- forget_shift: float32 [8, 8, 1024], P(('grp', 'sp'), 'tp'), parts along dimension 0, may hold values from 0 to 10.1
- new_query: bfloat16 [8, 8, 128], P(('grp', 'sp'), 'tp'), parts along dimension 0, may hold values from 0.1 to 2
- new_key: bfloat16 [8, 8, 128], P(('grp', 'sp'), 'tp'), parts along dimension 0, may hold values from -6 to 6
- new_value: bfloat16 [8, 8, 128], P(('grp', 'sp'), 'tp'), parts along dimension 0, may hold values from -6 to 6
- new_input: float32 [8, 8], P(('grp', 'sp'), 'tp'), parts along dimension 0, may hold values from 2 to 6
- new_forget: float32 [8, 8], P(('grp', 'sp'), 'tp'), parts along dimension 0, may hold values from -1 to 3
Outputs:
- key_cache: bfloat16 [8, 8, 1024, 128], P(('grp', 'sp'), 'tp'), parts along dimension 0
- value_cache: bfloat16 [8, 8, 1024, 128], P(('grp', 'sp'), 'tp'), parts along dimension 0
- weight_cache: float32 [8, 8, 1024], P(('grp', 'sp'), 'tp'), parts along dimension 0
- first_read: bfloat16 [8, 8, 128], P(('grp', 'sp'), 'tp'), parts along dimension 0
There are 2 independent parts, one for each index of `grp`. A program takes and returns all parts, laid end to end along the dimension named above; an argument that names none is the same for every part. Nothing has to cross between parts.
All inputs are finite; a program needn't handle non-finite values.
Results may differ from a plain program's by a relative error of at most 0.012.
Values may be sent and summed in bfloat16 or wider, within the bound.
A program may use at most 64 MiB of HBM per device.

v0:
```python
import jax
import jax.numpy as jnp
from jax import lax
from jax.sharding import PartitionSpec as P

HEADS = 8
DK = 128
CONV = 4
epsilon = 1e-06


def shifted(block, axis, distance):
    devices = range(lax.axis_size(axis))
    route = [(i - distance, i) for i in devices if i - distance in devices]
    return lax.ppermute(block, axis, route)


def project_rows(
    token_rows, norm_gain, key_weight, value_weight, input_gate_weight, forget_gate_weight
):
    widened = token_rows.astype(jnp.float32)
    normed = (
        widened
        * lax.rsqrt(jnp.mean(widened * widened, axis=-1, keepdims=True) + epsilon)
        * norm_gain.astype(jnp.float32)
    ).astype(jnp.bfloat16)
    key_matrix = key_weight.reshape(key_weight.shape[0], HEADS, DK)
    value_matrix = value_weight.reshape(value_weight.shape[0], HEADS, DK)
    key_linear = jnp.einsum(
        "apd,dhk->ahpk", normed, key_matrix, preferred_element_type=jnp.float32
    ).astype(jnp.bfloat16)
    values = jnp.einsum(
        "apd,dhk->ahpk", normed, value_matrix, preferred_element_type=jnp.float32
    ).astype(jnp.bfloat16)
    input_linear = jnp.einsum(
        "apd,dh->ahp", normed, input_gate_weight, preferred_element_type=jnp.float32
    ).astype(jnp.bfloat16)
    forget_linear = jnp.einsum(
        "apd,dh->ahp", normed, forget_gate_weight, preferred_element_type=jnp.float32
    ).astype(jnp.bfloat16)
    return (key_linear, values, input_linear, forget_linear)


def convolve(key_linear, previous, conv_weight):
    extended = jnp.concatenate([previous, key_linear], axis=2).astype(jnp.float32)
    length = key_linear.shape[2]
    tap_weight = conv_weight.reshape(CONV, HEADS, 1, DK)
    summed = extended[:, :, 0:length, :] * tap_weight[0]
    for offset in range(1, CONV):
        summed = summed + extended[:, :, offset : offset + length, :] * tap_weight[offset]
    return jax.nn.silu(summed).astype(jnp.bfloat16)


def read_cache(
    keys,
    values,
    input_linear,
    forget_linear,
    input_shift,
    forget_shift,
    new_query,
    new_key,
    new_value,
    new_input,
    new_forget,
):
    scaling = DK ** (-0.5)
    log_forget = jax.nn.log_sigmoid(forget_linear.astype(jnp.float32) + forget_shift)
    suffix = lax.cumsum(log_forget, axis=2, reverse=True) - log_forget
    new_decay = jax.nn.log_sigmoid(new_forget)
    log_weight = input_linear.astype(jnp.float32) + input_shift + suffix + new_decay[:, :, None]
    largest = jnp.maximum(jnp.max(log_weight, axis=2), new_input)
    weight_cache = jnp.exp(log_weight - largest[:, :, None])
    new_weight = jnp.exp(new_input - largest)
    matched = jnp.einsum("bhlk,bhk->bhl", keys, new_query, preferred_element_type=jnp.float32)
    scores = (weight_cache * matched * scaling).astype(jnp.bfloat16)
    fresh_match = jnp.sum(new_key.astype(jnp.float32) * new_query.astype(jnp.float32), axis=2)
    new_score = (new_weight * fresh_match * scaling).astype(jnp.bfloat16)
    denominator = jnp.sum(scores.astype(jnp.float32), axis=2) + new_score.astype(jnp.float32)
    numerator = jnp.einsum("bhl,bhlk->bhk", scores, values, preferred_element_type=jnp.float32)
    numerator = numerator + new_score.astype(jnp.float32)[:, :, None] * new_value.astype(
        jnp.float32
    )
    first_read = (numerator / jnp.maximum(jnp.abs(denominator), 1.0)[:, :, None]).astype(
        jnp.bfloat16
    )
    return (weight_cache, first_read)


def shards(
    layer_input,
    norm_gain,
    key_weight,
    value_weight,
    input_gate_weight,
    forget_gate_weight,
    conv_weight,
    input_shift,
    forget_shift,
    new_query,
    new_key,
    new_value,
    new_input,
    new_forget,
):
    key_linear, values, input_linear, forget_linear = project_rows(
        layer_input, norm_gain, key_weight, value_weight, input_gate_weight, forget_gate_weight
    )
    previous = shifted(key_linear[:, :, -(CONV - 1) :, :], "sp", 1)
    keys = convolve(key_linear, previous, conv_weight)
    keys, values, input_linear, forget_linear = (
        lax.all_to_all(
            lax.all_to_all(keys, "tp", split_axis=1, concat_axis=0, tiled=True),
            "sp",
            split_axis=0,
            concat_axis=2,
            tiled=True,
        ),
        lax.all_to_all(
            lax.all_to_all(values, "tp", split_axis=1, concat_axis=0, tiled=True),
            "sp",
            split_axis=0,
            concat_axis=2,
            tiled=True,
        ),
        lax.all_to_all(
            lax.all_to_all(input_linear, "tp", split_axis=1, concat_axis=0, tiled=True),
            "sp",
            split_axis=0,
            concat_axis=2,
            tiled=True,
        ),
        lax.all_to_all(
            lax.all_to_all(forget_linear, "tp", split_axis=1, concat_axis=0, tiled=True),
            "sp",
            split_axis=0,
            concat_axis=2,
            tiled=True,
        ),
    )
    weight_cache, first_read = read_cache(
        keys,
        values,
        input_linear,
        forget_linear,
        input_shift,
        forget_shift,
        new_query,
        new_key,
        new_value,
        new_input,
        new_forget,
    )
    return (keys, values, weight_cache, first_read)


def solution(mesh):
    in_specs = (
        P(("grp", "tp"), "sp", None),
        P(),
        P(),
        P(),
        P(),
        P(),
        P(),
        P(("grp", "sp"), "tp", None),
        P(("grp", "sp"), "tp", None),
        P(("grp", "sp"), "tp", None),
        P(("grp", "sp"), "tp", None),
        P(("grp", "sp"), "tp", None),
        P(("grp", "sp"), "tp"),
        P(("grp", "sp"), "tp"),
    )
    out_specs = (
        P(("grp", "sp"), "tp", None, None),
        P(("grp", "sp"), "tp", None, None),
        P(("grp", "sp"), "tp", None),
        P(("grp", "sp"), "tp", None),
    )
    return jax.shard_map(shards, mesh=mesh, in_specs=in_specs, out_specs=out_specs, check_vma=False)
```

profile of v0, /device:TPU:0, one launch (start us, length us, event | category | flops | bytes accessed | tf_op | source)
XLA Modules:
  0.0 106.6 jit_solution(14466072062410166473)
XLA Ops:
  1.4 1.5 %fusion.6 = f32[256]{0:T(256)S(1)} fusion(bf16[1,256,2048]{2,1,0:T(8,128)(2,1)} %param.14), kind=kLoop, calls=%fused_computation.8 | loop fusion | flops 1572608 | bytes 1049600 | tf_op jit(solution)/shard_map/reduce_sum | solution.py:24
  3.0 1.7 %fusion.22 = bf16[1,8,256]{2,1,0:T(8,128)(2,1)S(1)} fusion(bf16[2048,8]{0,1:T(8,128)(2,1)S(1)} %copy-done, bf16[1,256,2048]{2,1,0:T(8,128)(2,1)} %param.14, f32[2048]{0:T(1024)S(1)} %convert_element_type.131, f32[256]{0:T(256)S(1)} %add_rsqrt_fusion), kind=kOutput, calls=%fused_computation.18 | convolution fusion | flops 10487808 | bytes 1094656 | tf_op jit(solution)/shard_map/apd,dh->ahp/dot_general | solution.py:38
  6.5 6.3 %all-to-all-start.6 = ((bf16[4,2,256]{2,1,0:T(2,128)(2,1)}), bf16[4,2,256]{2,1,0:T(2,128)(2,1)S(1)}, u32[]{:S(2)}, u32[]{:S(2)}) async-start(bf16[4,2,256]{2,1,0:T(2,128)(2,1)} %reshape.225), calls=%async_computation.6 | async-start | bytes 8192 | tf_op jit(solution)/shard_map/all_to_all | solution.py:134
  14.6 3.8 %all-to-all-done.6 = bf16[4,2,256]{2,1,0:T(2,128)(2,1)S(1)} async-done(((bf16[4,2,256]{2,1,0:T(2,128)(2,1)}), bf16[4,2,256]{2,1,0:T(2,128)(2,1)S(1)}, u32[]{:S(2)}, u32[]{:S(2)}) %all-to-all-start.6) | async-done | bytes 4128 | tf_op jit(solution)/shard_map/all_to_all | solution.py:134
  18.4 3.2 %all-to-all-start.4 = ((bf16[4,2,256]{2,1,0:T(2,128)(2,1)}), bf16[4,2,256]{2,1,0:T(2,128)(2,1)S(1)}, u32[]{:S(2)}, u32[]{:S(2)}) async-start(bf16[4,2,256]{2,1,0:T(2,128)(2,1)} %reshape.227), calls=%async_computation.4 | async-start | bytes 8192 | tf_op jit(solution)/shard_map/all_to_all | solution.py:127
  22.3 4.9 %all-to-all-done.4 = bf16[4,2,256]{2,1,0:T(2,128)(2,1)S(1)} async-done(((bf16[4,2,256]{2,1,0:T(2,128)(2,1)}), bf16[4,2,256]{2,1,0:T(2,128)(2,1)S(1)}, u32[]{:S(2)}, u32[]{:S(2)}) %all-to-all-start.4) | async-done | bytes 4128 | tf_op jit(solution)/shard_map/all_to_all | solution.py:127
  27.2 3.2 %all-to-all-start.7 = ((bf16[4,2,256]{2,1,0:T(2,128)(2,1)}), bf16[4,2,256]{2,1,0:T(2,128)(2,1)S(1)}, u32[]{:S(2)}, u32[]{:S(2)}) async-start(bf16[4,2,256]{2,1,0:T(2,128)(2,1)} %all_to_all.92), calls=%async_computation.7 | async-start | bytes 8192 | tf_op jit(solution)/shard_map/all_to_all | solution.py:133
  31.1 3.1 %all-to-all-done.7 = bf16[4,2,256]{2,1,0:T(2,128)(2,1)S(1)} async-done(((bf16[4,2,256]{2,1,0:T(2,128)(2,1)}), bf16[4,2,256]{2,1,0:T(2,128)(2,1)S(1)}, u32[]{:S(2)}, u32[]{:S(2)}) %all-to-all-start.7) | async-done | bytes 4128 | tf_op jit(solution)/shard_map/all_to_all | solution.py:133
  34.2 3.2 %all-to-all-start.5 = ((bf16[4,2,256]{2,1,0:T(2,128)(2,1)}), bf16[4,2,256]{2,1,0:T(2,128)(2,1)S(1)}, u32[]{:S(2)}, u32[]{:S(2)}) async-start(bf16[4,2,256]{2,1,0:T(2,128)(2,1)} %all_to_all.89), calls=%async_computation.5 | async-start | bytes 8192 | tf_op jit(solution)/shard_map/all_to_all | solution.py:126
  37.5 4.3 %fusion.15 = bf16[1,8,256,128]{3,2,0,1:T(8,128)(2,1)} fusion(bf16[1,256,2048]{2,1,0:T(8,128)(2,1)S(1)} %copy-done.3, f32[2048]{0:T(1024)S(1)} %convert_element_type.131, f32[256]{0:T(256)S(1)} %add_rsqrt_fusion, bf16[2048,1024]{1,0:T(8,128)(2,1)} %param.17), kind=kOutput, calls=%fused_computation.13 | convolution fusion | flops 1076101120 | bytes 5776384 | tf_op jit(solution)/shard_map/apd,dhk->ahpk/dot_general | solution.py:32
  41.8 4.1 %all-to-all-start.2 = ((bf16[1,8,256,128]{3,2,0,1:T(8,128)(2,1)}), bf16[1,8,256,128]{3,2,0,1:T(8,128)(2,1)}, u32[]{:S(2)}, u32[]{:S(2)}) async-start(bf16[1,8,256,128]{3,2,0,1:T(8,128)(2,1)} %fusion.15), calls=%async_computation.2 | async-start | bytes 1048576 | tf_op jit(solution)/shard_map/all_to_all | solution.py:120
  45.9 3.5 %fusion.18 = bf16[1,8,256,128]{3,2,1,0:T(8,128)(2,1)S(1)} fusion(bf16[1,256,2048]{2,1,0:T(8,128)(2,1)S(1)} %copy-done.3, f32[2048]{0:T(1024)S(1)} %convert_element_type.131, f32[256]{0:T(256)S(1)} %add_rsqrt_fusion, bf16[2048,1024]{1,0:T(8,128)(2,1)} %param.16), kind=kOutput, calls=%fused_computation.14 | convolution fusion | flops 1076101120 | bytes 5776384 | tf_op jit(solution)/shard_map/apd,dhk->ahpk/dot_general | solution.py:29
  49.4 2.4 %collective-permute-start = (bf16[1,8,3,128]{3,2,1,0:T(4,128)(2,1)S(1)}, bf16[1,8,3,128]{3,2,1,0:T(4,128)(2,1)S(1)}, u32[]{:S(2)}, u32[]{:S(2)}) collective-permute-start(bf16[1,8,3,128]{3,2,1,0:T(4,128)(2,1)S(1)} %slice.48), channel_id=1, source_target_pairs={{0,4},{4,8},{8,12},{1,5},{5,9},{9,13},{2,6},{6,10},{10,14},{3,7},{... | collective-permute-start | bytes 18440 | tf_op jit(solution)/shard_map/ppermute | solution.py:15
  51.8 0.8 collective-permute-done
  52.8 1.5 %fusion.30 = bf16[1,8,256,128]{3,2,0,1:T(8,128)(2,1)} fusion(f32[8,128]{1,0:T(8,128)S(1)} %bitcast.172, f32[1,8,259,128]{3,2,1,0:T(8,128)S(1)} %maximum_convert_fusion, f32[8,128]{1,0:T(8,128)S(1)} %bitcast.173, f32[8,128]{1,0:T(8,128)S(1)} %bitcast.171, f32[8,128]{1,0:T(8,128)S(1)} %bitcast.170), kind=kLoop, calls=%fused_computation.32 | loop fusion | flops 3145728 | bytes 4734976 | tf_op jit(solution)/shard_map/convert_element_type | solution.py:51
  54.2 7.1 %all-to-all-done.2 = bf16[1,8,256,128]{3,2,0,1:T(8,128)(2,1)} async-done(((bf16[1,8,256,128]{3,2,0,1:T(8,128)(2,1)}), bf16[1,8,256,128]{3,2,0,1:T(8,128)(2,1)}, u32[]{:S(2)}, u32[]{:S(2)}) %all-to-all-start.2) | async-done | bytes 524320 | tf_op jit(solution)/shard_map/all_to_all | solution.py:120
  61.4 4.1 %all-to-all-start = ((bf16[1,8,256,128]{3,2,0,1:T(8,128)(2,1)}), bf16[1,8,256,128]{3,2,0,1:T(8,128)(2,1)}, u32[]{:S(2)}, u32[]{:S(2)}) async-start(bf16[1,8,256,128]{3,2,0,1:T(8,128)(2,1)} %fusion.30), calls=%async_computation | async-start | bytes 1048576 | tf_op jit(solution)/shard_map/all_to_all | solution.py:113
  65.7 2.5 %reduce-window.6 = f32[1,2,8,128]{3,2,1,0:T(8,128)S(1)} reduce-window(f32[1,2,8,128]{3,2,1,0:T(8,128)S(1)} %copy.82, f32[]{:T(128)} %constant.7.clone.1), window={size=1x1x1x128 pad=0_0x0_0x0_0x0_127}, to_apply=%region_1.2 | reduce-window | flops 260096 | bytes 16388 | tf_op jit(solution)/shard_map/reduce-window
  68.5 11.6 %all-to-all-done = bf16[1,8,256,128]{3,2,0,1:T(8,128)(2,1)} async-done(((bf16[1,8,256,128]{3,2,0,1:T(8,128)(2,1)}), bf16[1,8,256,128]{3,2,0,1:T(8,128)(2,1)}, u32[]{:S(2)}, u32[]{:S(2)}) %all-to-all-start) | async-done | bytes 524320 | tf_op jit(solution)/shard_map/all_to_all | solution.py:113
  80.1 3.5 %all-to-all-start.3 = ((bf16[4,2,256,128]{3,2,1,0:T(8,128)(2,1)}), bf16[4,2,256,128]{3,2,1,0:T(8,128)(2,1)S(1)}, u32[]{:S(2)}, u32[]{:S(2)}) async-start(bf16[4,2,256,128]{3,2,1,0:T(8,128)(2,1)} %bitcast.18), calls=%async_computation.3 | async-start | bytes 1048576 | tf_op jit(solution)/shard_map/all_to_all | solution.py:119
  83.7 8.6 %all-to-all-done.3 = bf16[4,2,256,128]{3,2,1,0:T(8,128)(2,1)S(1)} async-done(((bf16[4,2,256,128]{3,2,1,0:T(8,128)(2,1)}), bf16[4,2,256,128]{3,2,1,0:T(8,128)(2,1)S(1)}, u32[]{:S(2)}, u32[]{:S(2)}) %all-to-all-start.3) | async-done | bytes 524320 | tf_op jit(solution)/shard_map/all_to_all | solution.py:119
  92.3 3.6 %all-to-all-start.1 = ((bf16[4,2,256,128]{3,2,1,0:T(8,128)(2,1)}), bf16[4,2,256,128]{3,2,1,0:T(8,128)(2,1)S(1)}, u32[]{:S(2)}, u32[]{:S(2)}) async-start(bf16[4,2,256,128]{3,2,1,0:T(8,128)(2,1)} %bitcast.10), calls=%async_computation.1 | async-start | bytes 1048576 | tf_op jit(solution)/shard_map/all_to_all | solution.py:112
  96.2 8.5 %all-to-all-done.1 = bf16[4,2,256,128]{3,2,1,0:T(8,128)(2,1)S(1)} async-done(((bf16[4,2,256,128]{3,2,1,0:T(8,128)(2,1)}), bf16[4,2,256,128]{3,2,1,0:T(8,128)(2,1)S(1)}, u32[]{:S(2)}, u32[]{:S(2)}) %all-to-all-start.1) | async-done | bytes 524320 | tf_op jit(solution)/shard_map/all_to_all | solution.py:112
  105.0 0.8 convert_reduce_fusion
  (66 shorter events, 7.7 us)
Async XLA Ops:
  0.6 2.3 %copy-start = (bf16[2048,8]{0,1:T(8,128)(2,1)S(1)}, bf16[2048,8]{0,1:T(8,128)(2,1)}, u32[]{:S(2)}) copy-start(bf16[2048,8]{0,1:T(8,128)(2,1)} %param.19) | copy-start | bytes 98308
  0.6 12.2 %copy-start.3 = (bf16[1,256,2048]{2,1,0:T(8,128)(2,1)S(1)}, bf16[1,256,2048]{2,1,0:T(8,128)(2,1)}, u32[]{:S(2)}) copy-start(bf16[1,256,2048]{2,1,0:T(8,128)(2,1)} %param.14) | copy-start | bytes 3145732
  0.7 12.2 %copy-start.10 = (bf16[2048,8]{0,1:T(8,128)(2,1)S(1)}, bf16[2048,8]{0,1:T(8,128)(2,1)}, u32[]{:S(2)}) copy-start(bf16[2048,8]{0,1:T(8,128)(2,1)} %param.18) | copy-start | bytes 98308
  6.5 11.9 %all-to-all-start.6 = ((bf16[4,2,256]{2,1,0:T(2,128)(2,1)}), bf16[4,2,256]{2,1,0:T(2,128)(2,1)S(1)}, u32[]{:S(2)}, u32[]{:S(2)}) async-start(bf16[4,2,256]{2,1,0:T(2,128)(2,1)} %reshape.225), calls=%async_computation.6 | async-start | bytes 8192 | tf_op jit(solution)/shard_map/all_to_all | solution.py:134
  18.4 8.8 %all-to-all-start.4 = ((bf16[4,2,256]{2,1,0:T(2,128)(2,1)}), bf16[4,2,256]{2,1,0:T(2,128)(2,1)S(1)}, u32[]{:S(2)}, u32[]{:S(2)}) async-start(bf16[4,2,256]{2,1,0:T(2,128)(2,1)} %reshape.227), calls=%async_computation.4 | async-start | bytes 8192 | tf_op jit(solution)/shard_map/all_to_all | solution.py:127
  27.2 7.0 %all-to-all-start.7 = ((bf16[4,2,256]{2,1,0:T(2,128)(2,1)}), bf16[4,2,256]{2,1,0:T(2,128)(2,1)S(1)}, u32[]{:S(2)}, u32[]{:S(2)}) async-start(bf16[4,2,256]{2,1,0:T(2,128)(2,1)} %all_to_all.92), calls=%async_computation.7 | async-start | bytes 8192 | tf_op jit(solution)/shard_map/all_to_all | solution.py:133
  34.2 7.5 %all-to-all-start.5 = ((bf16[4,2,256]{2,1,0:T(2,128)(2,1)}), bf16[4,2,256]{2,1,0:T(2,128)(2,1)S(1)}, u32[]{:S(2)}, u32[]{:S(2)}) async-start(bf16[4,2,256]{2,1,0:T(2,128)(2,1)} %all_to_all.89), calls=%async_computation.5 | async-start | bytes 8192 | tf_op jit(solution)/shard_map/all_to_all | solution.py:126
  41.8 19.6 %all-to-all-start.2 = ((bf16[1,8,256,128]{3,2,0,1:T(8,128)(2,1)}), bf16[1,8,256,128]{3,2,0,1:T(8,128)(2,1)}, u32[]{:S(2)}, u32[]{:S(2)}) async-start(bf16[1,8,256,128]{3,2,0,1:T(8,128)(2,1)} %fusion.15), calls=%async_computation.2 | async-start | bytes 1048576 | tf_op jit(solution)/shard_map/all_to_all | solution.py:120
  45.9 5.9 %copy-start.5 = (f32[4,1024]{1,0:T(4,128)S(1)}, f32[4,1024]{1,0:T(4,128)}, u32[]{:S(2)}) copy-start(f32[4,1024]{1,0:T(4,128)} %param.20) | copy-start | bytes 49156
  49.4 3.2 %collective-permute-start = (bf16[1,8,3,128]{3,2,1,0:T(4,128)(2,1)S(1)}, bf16[1,8,3,128]{3,2,1,0:T(4,128)(2,1)S(1)}, u32[]{:S(2)}, u32[]{:S(2)}) collective-permute-start(bf16[1,8,3,128]{3,2,1,0:T(4,128)(2,1)S(1)} %slice.48), channel_id=1, source_target_pairs={{0,4},{4,8},{8,12},{1,5},{5,9},{9,13},{2,6},{6,10},{10,14},{3,7},{... | collective-permute-start | bytes 18440 | tf_op jit(solution)/shard_map/ppermute | solution.py:15
  52.7 12.8 %copy-start.7 = (bf16[1,2,128]{2,1,0:T(2,128)(2,1)S(1)}, bf16[1,2,128]{2,1,0:T(2,128)(2,1)}, u32[]{:S(2)}) copy-start(bf16[1,2,128]{2,1,0:T(2,128)(2,1)} %param.23) | copy-start | bytes 1540
  52.7 12.8 %copy-start.11 = (bf16[1,2,128]{2,1,0:T(2,128)(2,1)S(1)}, bf16[1,2,128]{2,1,0:T(2,128)(2,1)}, u32[]{:S(2)}) copy-start(bf16[1,2,128]{2,1,0:T(2,128)(2,1)} %param.24) | copy-start | bytes 1540
  52.8 12.9 %copy-start.12 = (f32[1,2]{1,0:T(1,128)S(1)}, f32[1,2]{1,0:T(1,128)}, u32[]{:S(2)}) copy-start(f32[1,2]{1,0:T(1,128)} %param.27) | copy-start | bytes 28
  52.8 12.9 %copy-start.4 = (f32[1,2,1024]{2,1,0:T(2,128)S(1)}, f32[1,2,1024]{2,1,0:T(2,128)}, u32[]{:S(2)}) copy-start(f32[1,2,1024]{2,1,0:T(2,128)} %param.22) | copy-start | bytes 24580
  54.2 41.7 %copy-start.6 = (f32[1,2,1024]{2,1,0:T(2,128)S(1)}, f32[1,2,1024]{2,1,0:T(2,128)}, u32[]{:S(2)}) copy-start(f32[1,2,1024]{2,1,0:T(2,128)} %param.21) | copy-start | bytes 24580
  54.2 41.9 %copy-start.8 = (f32[1,2]{1,0:T(1,128)S(1)}, f32[1,2]{1,0:T(1,128)}, u32[]{:S(2)}) copy-start(f32[1,2]{1,0:T(1,128)} %param.26) | copy-start | bytes 28
  61.4 18.7 %all-to-all-start = ((bf16[1,8,256,128]{3,2,0,1:T(8,128)(2,1)}), bf16[1,8,256,128]{3,2,0,1:T(8,128)(2,1)}, u32[]{:S(2)}, u32[]{:S(2)}) async-start(bf16[1,8,256,128]{3,2,0,1:T(8,128)(2,1)} %fusion.30), calls=%async_computation | async-start | bytes 1048576 | tf_op jit(solution)/shard_map/all_to_all | solution.py:113
  80.1 12.3 %all-to-all-start.3 = ((bf16[4,2,256,128]{3,2,1,0:T(8,128)(2,1)}), bf16[4,2,256,128]{3,2,1,0:T(8,128)(2,1)S(1)}, u32[]{:S(2)}, u32[]{:S(2)}) async-start(bf16[4,2,256,128]{3,2,1,0:T(8,128)(2,1)} %bitcast.18), calls=%async_computation.3 | async-start | bytes 1048576 | tf_op jit(solution)/shard_map/all_to_all | solution.py:119
  92.3 13.7 %copy-start.9 = (bf16[1,2,128]{2,1,0:T(2,128)(2,1)S(1)}, bf16[1,2,128]{2,1,0:T(2,128)(2,1)}, u32[]{:S(2)}) copy-start(bf16[1,2,128]{2,1,0:T(2,128)(2,1)} %param.25) | copy-start | bytes 1540
  92.3 12.4 %all-to-all-start.1 = ((bf16[4,2,256,128]{3,2,1,0:T(8,128)(2,1)}), bf16[4,2,256,128]{3,2,1,0:T(8,128)(2,1)S(1)}, u32[]{:S(2)}, u32[]{:S(2)}) async-start(bf16[4,2,256,128]{3,2,1,0:T(8,128)(2,1)} %bitcast.10), calls=%async_computation.1 | async-start | bytes 1048576 | tf_op jit(solution)/shard_map/all_to_all | solution.py:112
  96.2 10.4 %copy-start.1 = (bf16[4,2,256,128]{3,2,0,1:T(8,128)(2,1)}, bf16[4,2,256,128]{3,2,0,1:T(8,128)(2,1)S(1)}, u32[]{:S(2)}) copy-start(bf16[4,2,256,128]{3,2,0,1:T(8,128)(2,1)S(1)} %copy.45) | copy-start | bytes 1572868
  104.8 1.9 %copy-start.2 = (bf16[4,2,256,128]{3,2,0,1:T(8,128)(2,1)}, bf16[4,2,256,128]{3,2,0,1:T(8,128)(2,1)S(1)}, u32[]{:S(2)}) copy-start(bf16[4,2,256,128]{3,2,0,1:T(8,128)(2,1)S(1)} %copy.42) | copy-start | bytes 1572868
where the time goes:
time: 107 us
  waiting for transfers between devices  48.4 us (45%)
  starting transfers between devices  33.8 us (32%)
  matrix products  10.3 us (10%)
  other arithmetic  9.68 us (9%)
  local copies, waits for them, and re-layouts  3.49 us (3%)
    all_to_all x1, waiting for transfers between devices, shards(): lax.all_to_all(keys, 'tp', split_axis=1, concat_axis=0, tiled=True)  11.6 us
    all_to_all x1, waiting for transfers between devices, shards(): lax.all_to_all(lax.all_to_all(values, 'tp', split_axis=1, concat_axis=0,...  8.61 us
    all_to_all x1, waiting for transfers between devices, shards(): lax.all_to_all(lax.all_to_all(keys, 'tp', split_axis=1, concat_axis=0, ti...  8.51 us
    all_to_all x1, waiting for transfers between devices, shards(): lax.all_to_all(values, 'tp', split_axis=1, concat_axis=0, tiled=True)  7.12 us
    all_to_all x1, starting transfers between devices, shards(): lax.all_to_all(forget_linear, 'tp', split_axis=1, concat_axis=0, tiled=True)  6.35 us
    all_to_all x1, waiting for transfers between devices, shards(): lax.all_to_all(input_linear, 'tp', split_axis=1, concat_axis=0, tiled=True)  4.89 us
    dot_general x1, matrix products, project_rows(): jnp.einsum('apd,dhk->ahpk', normed, value_matrix, preferred_element_type=...  4.29 us
    all_to_all x1, starting transfers between devices, shards(): lax.all_to_all(values, 'tp', split_axis=1, concat_axis=0, tiled=True)  4.14 us
  transfers between devices with their start and end apart: 9, of which 8 were waited for; matrix products, arithmetic and copies ran while one was open for 14% of the time, Pallas kernels for 0%

commit v1 on v0

--- a/solution.py
+++ b/solution.py
@@ -7,6 +7,22 @@
 DK = 128
 CONV = 4
 epsilon = 1e-06
+
+
+def swapped_with_each(x, axis, split, join):
+    ways, here = (lax.axis_size(axis), lax.axis_index(axis))
+    width = x.shape[split] // ways
+    shape = list(x.shape)
+    shape[split] = width
+    height = shape[join]
+    shape[join] = height * ways
+    full = jnp.zeros(shape, x.dtype)
+    for mask in range(ways):
+        part = lax.dynamic_slice_in_dim(x, (here ^ mask) * width, width, axis=split)
+        if mask:
+            part = lax.ppermute(part, axis, [(d, d ^ mask) for d in range(ways)])
+        full = lax.dynamic_update_slice_in_dim(full, part, (here ^ mask) * height, axis=join)
+    return full
 
 
 def shifted(block, axis, distance):
@@ -124,7 +140,7 @@
             tiled=True,
         ),
         lax.all_to_all(
-            lax.all_to_all(input_linear, "tp", split_axis=1, concat_axis=0, tiled=True),
+            swapped_with_each(input_linear, "tp", 1, 0),
             "sp",
             split_axis=0,
             concat_axis=2,

time: 107 us -> 104 us (0.972)
  waiting for transfers between devices: 48.4 us -> 42.7 us
  local copies, waits for them, and re-layouts: 3.49 us -> 5.1 us
  starting transfers between devices: 33.8 us -> 35.1 us
    ppermute x0 -> x3, starting transfers between devices: none -> 4.53 us  [swapped_with_each(): part = lax.ppermute(part, axis, [(d, d ^ mask) for d in range(ways)])]
    all_to_all x1, waiting for transfers between devices: 3.82 us -> 0.01 us  [shards(): lax.all_to_all(forget_linear, 'tp', split_axis=1, concat_axis=0, tiled=True)]
    all_to_all x2 -> x1, starting transfers between devices: 6.49 us -> 3.25 us  [shards(): lax.all_to_all(swapped_with_each(input_linear, 'tp', 1, 0), 'sp', split_a...]
    all_to_all x1, waiting for transfers between devices: 3.1 us -> 0.01 us  [shards(): lax.all_to_all(lax.all_to_all(forget_linear, 'tp', split_axis=1, concat_a...]
    ppermute x0 -> x3, waiting for transfers between devices: none -> 3 us  [swapped_with_each(): part = lax.ppermute(part, axis, [(d, d ^ mask) for d in range(ways)])]
    all_to_all x1, waiting for transfers between devices: 8.61 us -> 5.78 us  [shards(): lax.all_to_all(lax.all_to_all(values, 'tp', split_axis=1, concat_axis=0,...]
    all_to_all x1, waiting for transfers between devices: 11.6 us -> 14.4 us  [shards(): lax.all_to_all(keys, 'tp', split_axis=1, concat_axis=0, tiled=True)]
    dynamic_update_slice x0 -> x4, local copies, waits for them, and re-layouts: none -> 2.26 us  [swapped_with_each(): lax.dynamic_update_slice_in_dim(full, part, (here ^ mask) * height, axis=...]
  transfers between devices with their start and end apart: 9 -> 11, of which waited for: 8 -> 8; matrix products, arithmetic and copies ran while one was open for 14% -> 16% of each run, Pallas kernels for 0% -> 0%
where the time goes in v1:
time: 104 us; the launch traced here: 103 us
  waiting for transfers between devices  42.7 us (41%)
  starting transfers between devices  35.1 us (34%)
  matrix products  10.3 us (10%)
  other arithmetic  9 us (9%)
  local copies, waits for them, and re-layouts  5.1 us (5%)
    all_to_all x1, waiting for transfers between devices, shards(): lax.all_to_all(keys, 'tp', split_axis=1, concat_axis=0, tiled=True)  14.4 us
    all_to_all x1, waiting for transfers between devices, shards(): lax.all_to_all(lax.all_to_all(keys, 'tp', split_axis=1, concat_axis=0, ti...  8.51 us
    all_to_all x1, waiting for transfers between devices, shards(): lax.all_to_all(values, 'tp', split_axis=1, concat_axis=0, tiled=True)  7.11 us
    all_to_all x1, starting transfers between devices, shards(): lax.all_to_all(forget_linear, 'tp', split_axis=1, concat_axis=0, tiled=True)  6.35 us
    all_to_all x1, waiting for transfers between devices, shards(): lax.all_to_all(lax.all_to_all(values, 'tp', split_axis=1, concat_axis=0,...  5.78 us
    ppermute x3, starting transfers between devices, swapped_with_each(): part = lax.ppermute(part, axis, [(d, d ^ mask) for d in range(ways)])  4.53 us
    dot_general x1, matrix products, project_rows(): jnp.einsum('apd,dhk->ahpk', normed, value_matrix, preferred_element_type=...  4.3 us
    all_to_all x1, starting transfers between devices, shards(): lax.all_to_all(keys, 'tp', split_axis=1, concat_axis=0, tiled=True)  4.14 us
  transfers between devices with their start and end apart: 11, of which 8 were waited for; matrix products, arithmetic and copies ran while one was open for 16% of the time, Pallas kernels for 0%

profile of v1, /device:TPU:0, one launch (start us, length us, event | category | flops | bytes accessed | tf_op | source)
XLA Modules:
  0.0 103.1 jit_solution(10686705724904647023)
XLA Ops:
  1.4 1.5 %fusion.6 = f32[256]{0:T(256)S(1)} fusion(bf16[1,256,2048]{2,1,0:T(8,128)(2,1)} %param.14), kind=kLoop, calls=%fused_computation.8 | loop fusion | flops 1572608 | bytes 1049600 | tf_op jit(solution)/shard_map/reduce_sum | solution.py:40
  3.0 1.7 %fusion.21 = bf16[1,8,256]{2,1,0:T(8,128)(2,1)S(1)} fusion(bf16[2048,8]{0,1:T(8,128)(2,1)S(1)} %copy-done, bf16[1,256,2048]{2,1,0:T(8,128)(2,1)} %param.14, f32[2048]{0:T(1024)S(1)} %convert_element_type.127, f32[256]{0:T(256)S(1)} %add_rsqrt_fusion), kind=kOutput, calls=%fused_computation.17 | convolution fusion | flops 10487808 | bytes 1094656 | tf_op jit(solution)/shard_map/apd,dh->ahp/dot_general | solution.py:54
  6.5 6.3 %all-to-all-start.5 = ((bf16[4,2,256]{2,1,0:T(2,128)(2,1)}), bf16[4,2,256]{2,1,0:T(2,128)(2,1)S(1)}, u32[]{:S(2)}, u32[]{:S(2)}) async-start(bf16[4,2,256]{2,1,0:T(2,128)(2,1)} %reshape.225), calls=%async_computation.5 | async-start | bytes 8192 | tf_op jit(solution)/shard_map/all_to_all | solution.py:150
  13.3 2.1 %collective-permute-start.1 = (bf16[1,2,256]{2,1,0:T(2,128)(2,1)S(1)}, bf16[1,2,256]{2,1,0:T(2,128)(2,1)S(1)}, u32[]{:S(2)}, u32[]{:S(2)}) collective-permute-start(bf16[1,2,256]{2,1,0:T(2,128)(2,1)S(1)} %get-tuple-element.17), channel_id=1, source_target_pairs={{0,1},{1,0},{2,3},{3,2},{4,5},{5,4},{6,7},{7,6},{8,9},{9,8},{10,11... | collective-permute-start | bytes 3080 | tf_op jit(solution)/shard_map/ppermute | solution.py:23
  15.4 2.4 %collective-permute-start.2 = (bf16[1,2,256]{2,1,0:T(2,128)(2,1)S(1)}, bf16[1,2,256]{2,1,0:T(2,128)(2,1)S(1)}, u32[]{:S(2)}, u32[]{:S(2)}) collective-permute-start(bf16[1,2,256]{2,1,0:T(2,128)(2,1)S(1)} %get-tuple-element.16), channel_id=1, source_target_pairs={{0,2},{1,3},{2,0},{3,1},{4,6},{5,7},{6,4},{7,5},{8,10},{9,11},{10,... | collective-permute-start | bytes 3080 | tf_op jit(solution)/shard_map/ppermute | solution.py:23
  20.4 2.7 %collective-permute-done.3 = bf16[1,2,256]{2,1,0:T(2,128)(2,1)S(1)} collective-permute-done((bf16[1,2,256]{2,1,0:T(2,128)(2,1)S(1)}, bf16[1,2,256]{2,1,0:T(2,128)(2,1)S(1)}, u32[]{:S(2)}, u32[]{:S(2)}) %collective-permute-start.3) | collective-permute-done | bytes 1056 | tf_op jit(solution)/shard_map/ppermute | solution.py:23
  23.7 3.2 %all-to-all-start.4 = ((bf16[4,2,256]{2,1,0:T(2,128)(2,1)}), bf16[4,2,256]{2,1,0:T(2,128)(2,1)S(1)}, u32[]{:S(2)}, u32[]{:S(2)}) async-start(bf16[4,2,256]{2,1,0:T(2,128)(2,1)} %constant_dynamic-update-slice_fusion), calls=%async_computation.4 | async-start | bytes 8192 | tf_op jit(solution)/shard_map/all_to_all | solution.py:142
  27.6 3.1 %all-to-all-done.4 = bf16[4,2,256]{2,1,0:T(2,128)(2,1)S(1)} async-done(((bf16[4,2,256]{2,1,0:T(2,128)(2,1)}), bf16[4,2,256]{2,1,0:T(2,128)(2,1)S(1)}, u32[]{:S(2)}, u32[]{:S(2)}) %all-to-all-start.4) | async-done | bytes 4128 | tf_op jit(solution)/shard_map/all_to_all | solution.py:142
  30.7 3.2 %all-to-all-start.6 = ((bf16[4,2,256]{2,1,0:T(2,128)(2,1)}), bf16[4,2,256]{2,1,0:T(2,128)(2,1)S(1)}, u32[]{:S(2)}, u32[]{:S(2)}) async-start(bf16[4,2,256]{2,1,0:T(2,128)(2,1)} %all_to_all.81), calls=%async_computation.6 | async-start | bytes 8192 | tf_op jit(solution)/shard_map/all_to_all | solution.py:149
  34.0 4.3 %fusion.15 = bf16[1,8,256,128]{3,2,0,1:T(8,128)(2,1)} fusion(bf16[1,256,2048]{2,1,0:T(8,128)(2,1)S(1)} %copy-done.3, f32[2048]{0:T(1024)S(1)} %convert_element_type.127, f32[256]{0:T(256)S(1)} %add_rsqrt_fusion, bf16[2048,1024]{1,0:T(8,128)(2,1)} %param.17), kind=kOutput, calls=%fused_computation.13 | convolution fusion | flops 1076101120 | bytes 5776384 | tf_op jit(solution)/shard_map/apd,dhk->ahpk/dot_general | solution.py:48
  38.3 4.1 %all-to-all-start.2 = ((bf16[1,8,256,128]{3,2,0,1:T(8,128)(2,1)}), bf16[1,8,256,128]{3,2,0,1:T(8,128)(2,1)}, u32[]{:S(2)}, u32[]{:S(2)}) async-start(bf16[1,8,256,128]{3,2,0,1:T(8,128)(2,1)} %fusion.15), calls=%async_computation.2 | async-start | bytes 1048576 | tf_op jit(solution)/shard_map/all_to_all | solution.py:136
  42.4 3.5 %fusion.18 = bf16[1,8,256,128]{3,2,1,0:T(8,128)(2,1)S(1)} fusion(bf16[1,256,2048]{2,1,0:T(8,128)(2,1)S(1)} %copy-done.3, f32[2048]{0:T(1024)S(1)} %convert_element_type.127, f32[256]{0:T(256)S(1)} %add_rsqrt_fusion, bf16[2048,1024]{1,0:T(8,128)(2,1)} %param.16), kind=kOutput, calls=%fused_computation.14 | convolution fusion | flops 1076101120 | bytes 5776384 | tf_op jit(solution)/shard_map/apd,dhk->ahpk/dot_general | solution.py:45
  45.9 2.4 %collective-permute-start = (bf16[1,8,3,128]{3,2,1,0:T(4,128)(2,1)S(1)}, bf16[1,8,3,128]{3,2,1,0:T(4,128)(2,1)S(1)}, u32[]{:S(2)}, u32[]{:S(2)}) collective-permute-start(bf16[1,8,3,128]{3,2,1,0:T(4,128)(2,1)S(1)} %slice.48), channel_id=1, source_target_pairs={{0,4},{4,8},{8,12},{1,5},{5,9},{9,13},{2,6},{6,10},{10,14},{3,7},{... | collective-permute-start | bytes 18440 | tf_op jit(solution)/shard_map/ppermute | solution.py:31
  48.3 0.8 collective-permute-done
  49.3 1.5 %fusion.29 = bf16[1,8,256,128]{3,2,0,1:T(8,128)(2,1)} fusion(f32[8,128]{1,0:T(8,128)S(1)} %bitcast.180, f32[1,8,259,128]{3,2,1,0:T(8,128)S(1)} %maximum_convert_fusion, f32[8,128]{1,0:T(8,128)S(1)} %bitcast.181, f32[8,128]{1,0:T(8,128)S(1)} %bitcast.179, f32[8,128]{1,0:T(8,128)S(1)} %bitcast.178), kind=kLoop, calls=%fused_computation.31 | loop fusion | flops 3145728 | bytes 4734976 | tf_op jit(solution)/shard_map/convert_element_type | solution.py:67
  50.7 7.1 %all-to-all-done.2 = bf16[1,8,256,128]{3,2,0,1:T(8,128)(2,1)} async-done(((bf16[1,8,256,128]{3,2,0,1:T(8,128)(2,1)}), bf16[1,8,256,128]{3,2,0,1:T(8,128)(2,1)}, u32[]{:S(2)}, u32[]{:S(2)}) %all-to-all-start.2) | async-done | bytes 524320 | tf_op jit(solution)/shard_map/all_to_all | solution.py:136
  57.8 4.1 %all-to-all-start = ((bf16[1,8,256,128]{3,2,0,1:T(8,128)(2,1)}), bf16[1,8,256,128]{3,2,0,1:T(8,128)(2,1)}, u32[]{:S(2)}, u32[]{:S(2)}) async-start(bf16[1,8,256,128]{3,2,0,1:T(8,128)(2,1)} %fusion.29), calls=%async_computation | async-start | bytes 1048576 | tf_op jit(solution)/shard_map/all_to_all | solution.py:129
  62.2 14.4 %all-to-all-done = bf16[1,8,256,128]{3,2,0,1:T(8,128)(2,1)} async-done(((bf16[1,8,256,128]{3,2,0,1:T(8,128)(2,1)}), bf16[1,8,256,128]{3,2,0,1:T(8,128)(2,1)}, u32[]{:S(2)}, u32[]{:S(2)}) %all-to-all-start) | async-done | bytes 524320 | tf_op jit(solution)/shard_map/all_to_all | solution.py:129
  76.6 3.5 %all-to-all-start.3 = ((bf16[4,2,256,128]{3,2,1,0:T(8,128)(2,1)}), bf16[4,2,256,128]{3,2,1,0:T(8,128)(2,1)S(1)}, u32[]{:S(2)}, u32[]{:S(2)}) async-start(bf16[4,2,256,128]{3,2,1,0:T(8,128)(2,1)} %bitcast.18), calls=%async_computation.3 | async-start | bytes 1048576 | tf_op jit(solution)/shard_map/all_to_all | solution.py:135
  80.1 2.5 %reduce-window.6 = f32[1,2,8,128]{3,2,1,0:T(8,128)S(1)} reduce-window(f32[1,2,8,128]{3,2,1,0:T(8,128)S(1)} %copy.75, f32[]{:T(128)} %constant.14.clone.1), window={size=1x1x1x128 pad=0_0x0_0x0_0x0_127}, to_apply=%region_1.2 | reduce-window | flops 260096 | bytes 16388 | tf_op jit(solution)/shard_map/reduce-window
  83.1 5.8 %all-to-all-done.3 = bf16[4,2,256,128]{3,2,1,0:T(8,128)(2,1)S(1)} async-done(((bf16[4,2,256,128]{3,2,1,0:T(8,128)(2,1)}), bf16[4,2,256,128]{3,2,1,0:T(8,128)(2,1)S(1)}, u32[]{:S(2)}, u32[]{:S(2)}) %all-to-all-start.3) | async-done | bytes 524320 | tf_op jit(solution)/shard_map/all_to_all | solution.py:135
  88.8 3.6 %all-to-all-start.1 = ((bf16[4,2,256,128]{3,2,1,0:T(8,128)(2,1)}), bf16[4,2,256,128]{3,2,1,0:T(8,128)(2,1)S(1)}, u32[]{:S(2)}, u32[]{:S(2)}) async-start(bf16[4,2,256,128]{3,2,1,0:T(8,128)(2,1)} %bitcast.10), calls=%async_computation.1 | async-start | bytes 1048576 | tf_op jit(solution)/shard_map/all_to_all | solution.py:128
  92.7 8.5 %all-to-all-done.1 = bf16[4,2,256,128]{3,2,1,0:T(8,128)(2,1)S(1)} async-done(((bf16[4,2,256,128]{3,2,1,0:T(8,128)(2,1)}), bf16[4,2,256,128]{3,2,1,0:T(8,128)(2,1)S(1)}, u32[]{:S(2)}, u32[]{:S(2)}) %all-to-all-start.1) | async-done | bytes 524320 | tf_op jit(solution)/shard_map/all_to_all | solution.py:128
  101.5 0.8 convert_reduce_fusion
  (70 shorter events, 9.1 us)
Async XLA Ops:
  0.6 2.3 %copy-start = (bf16[2048,8]{0,1:T(8,128)(2,1)S(1)}, bf16[2048,8]{0,1:T(8,128)(2,1)}, u32[]{:S(2)}) copy-start(bf16[2048,8]{0,1:T(8,128)(2,1)} %param.19) | copy-start | bytes 98308
  0.6 12.2 %copy-start.3 = (bf16[1,256,2048]{2,1,0:T(8,128)(2,1)S(1)}, bf16[1,256,2048]{2,1,0:T(8,128)(2,1)}, u32[]{:S(2)}) copy-start(bf16[1,256,2048]{2,1,0:T(8,128)(2,1)} %param.14) | copy-start | bytes 3145732
  0.7 12.2 %copy-start.10 = (bf16[2048,8]{0,1:T(8,128)(2,1)S(1)}, bf16[2048,8]{0,1:T(8,128)(2,1)}, u32[]{:S(2)}) copy-start(bf16[2048,8]{0,1:T(8,128)(2,1)} %param.18) | copy-start | bytes 98308
  6.5 17.2 %all-to-all-start.5 = ((bf16[4,2,256]{2,1,0:T(2,128)(2,1)}), bf16[4,2,256]{2,1,0:T(2,128)(2,1)S(1)}, u32[]{:S(2)}, u32[]{:S(2)}) async-start(bf16[4,2,256]{2,1,0:T(2,128)(2,1)} %reshape.225), calls=%async_computation.5 | async-start | bytes 8192 | tf_op jit(solution)/shard_map/all_to_all | solution.py:150
  13.3 5.7 %collective-permute-start.1 = (bf16[1,2,256]{2,1,0:T(2,128)(2,1)S(1)}, bf16[1,2,256]{2,1,0:T(2,128)(2,1)S(1)}, u32[]{:S(2)}, u32[]{:S(2)}) collective-permute-start(bf16[1,2,256]{2,1,0:T(2,128)(2,1)S(1)} %get-tuple-element.17), channel_id=1, source_target_pairs={{0,1},{1,0},{2,3},{3,2},{4,5},{5,4},{6,7},{7,6},{8,9},{9,8},{10,11... | collective-permute-start | bytes 3080 | tf_op jit(solution)/shard_map/ppermute | solution.py:23
  15.4 4.5 %collective-permute-start.2 = (bf16[1,2,256]{2,1,0:T(2,128)(2,1)S(1)}, bf16[1,2,256]{2,1,0:T(2,128)(2,1)S(1)}, u32[]{:S(2)}, u32[]{:S(2)}) collective-permute-start(bf16[1,2,256]{2,1,0:T(2,128)(2,1)S(1)} %get-tuple-element.16), channel_id=1, source_target_pairs={{0,2},{1,3},{2,0},{3,1},{4,6},{5,7},{6,4},{7,5},{8,10},{9,11},{10,... | collective-permute-start | bytes 3080 | tf_op jit(solution)/shard_map/ppermute | solution.py:23
  17.7 5.4 %collective-permute-start.3 = (bf16[1,2,256]{2,1,0:T(2,128)(2,1)S(1)}, bf16[1,2,256]{2,1,0:T(2,128)(2,1)S(1)}, u32[]{:S(2)}, u32[]{:S(2)}) collective-permute-start(bf16[1,2,256]{2,1,0:T(2,128)(2,1)S(1)} %get-tuple-element.15), channel_id=1, source_target_pairs={{0,3},{1,2},{2,1},{3,0},{4,7},{5,6},{6,5},{7,4},{8,11},{9,10},{10,... | collective-permute-start | bytes 3080 | tf_op jit(solution)/shard_map/ppermute | solution.py:23
  23.7 7.0 %all-to-all-start.4 = ((bf16[4,2,256]{2,1,0:T(2,128)(2,1)}), bf16[4,2,256]{2,1,0:T(2,128)(2,1)S(1)}, u32[]{:S(2)}, u32[]{:S(2)}) async-start(bf16[4,2,256]{2,1,0:T(2,128)(2,1)} %constant_dynamic-update-slice_fusion), calls=%async_computation.4 | async-start | bytes 8192 | tf_op jit(solution)/shard_map/all_to_all | solution.py:142
  30.7 7.6 %all-to-all-start.6 = ((bf16[4,2,256]{2,1,0:T(2,128)(2,1)}), bf16[4,2,256]{2,1,0:T(2,128)(2,1)S(1)}, u32[]{:S(2)}, u32[]{:S(2)}) async-start(bf16[4,2,256]{2,1,0:T(2,128)(2,1)} %all_to_all.81), calls=%async_computation.6 | async-start | bytes 8192 | tf_op jit(solution)/shard_map/all_to_all | solution.py:149
  38.3 19.6 %all-to-all-start.2 = ((bf16[1,8,256,128]{3,2,0,1:T(8,128)(2,1)}), bf16[1,8,256,128]{3,2,0,1:T(8,128)(2,1)}, u32[]{:S(2)}, u32[]{:S(2)}) async-start(bf16[1,8,256,128]{3,2,0,1:T(8,128)(2,1)} %fusion.15), calls=%async_computation.2 | async-start | bytes 1048576 | tf_op jit(solution)/shard_map/all_to_all | solution.py:136
  42.4 5.9 %copy-start.5 = (f32[4,1024]{1,0:T(4,128)S(1)}, f32[4,1024]{1,0:T(4,128)}, u32[]{:S(2)}) copy-start(f32[4,1024]{1,0:T(4,128)} %param.20) | copy-start | bytes 49156
  45.9 3.2 %collective-permute-start = (bf16[1,8,3,128]{3,2,1,0:T(4,128)(2,1)S(1)}, bf16[1,8,3,128]{3,2,1,0:T(4,128)(2,1)S(1)}, u32[]{:S(2)}, u32[]{:S(2)}) collective-permute-start(bf16[1,8,3,128]{3,2,1,0:T(4,128)(2,1)S(1)} %slice.48), channel_id=1, source_target_pairs={{0,4},{4,8},{8,12},{1,5},{5,9},{9,13},{2,6},{6,10},{10,14},{3,7},{... | collective-permute-start | bytes 18440 | tf_op jit(solution)/shard_map/ppermute | solution.py:31
  49.2 12.8 %copy-start.7 = (bf16[1,2,128]{2,1,0:T(2,128)(2,1)S(1)}, bf16[1,2,128]{2,1,0:T(2,128)(2,1)}, u32[]{:S(2)}) copy-start(bf16[1,2,128]{2,1,0:T(2,128)(2,1)} %param.23) | copy-start | bytes 1540
  49.2 12.8 %copy-start.11 = (bf16[1,2,128]{2,1,0:T(2,128)(2,1)S(1)}, bf16[1,2,128]{2,1,0:T(2,128)(2,1)}, u32[]{:S(2)}) copy-start(bf16[1,2,128]{2,1,0:T(2,128)(2,1)} %param.24) | copy-start | bytes 1540
  49.2 12.9 %copy-start.12 = (f32[1,2]{1,0:T(1,128)S(1)}, f32[1,2]{1,0:T(1,128)}, u32[]{:S(2)}) copy-start(f32[1,2]{1,0:T(1,128)} %param.27) | copy-start | bytes 28
  50.7 29.3 %copy-start.4 = (f32[1,2,1024]{2,1,0:T(2,128)S(1)}, f32[1,2,1024]{2,1,0:T(2,128)}, u32[]{:S(2)}) copy-start(f32[1,2,1024]{2,1,0:T(2,128)} %param.22) | copy-start | bytes 24580
  50.7 41.7 %copy-start.6 = (f32[1,2,1024]{2,1,0:T(2,128)S(1)}, f32[1,2,1024]{2,1,0:T(2,128)}, u32[]{:S(2)}) copy-start(f32[1,2,1024]{2,1,0:T(2,128)} %param.21) | copy-start | bytes 24580
  50.7 41.9 %copy-start.8 = (f32[1,2]{1,0:T(1,128)S(1)}, f32[1,2]{1,0:T(1,128)}, u32[]{:S(2)}) copy-start(f32[1,2]{1,0:T(1,128)} %param.26) | copy-start | bytes 28
  57.8 18.7 %all-to-all-start = ((bf16[1,8,256,128]{3,2,0,1:T(8,128)(2,1)}), bf16[1,8,256,128]{3,2,0,1:T(8,128)(2,1)}, u32[]{:S(2)}, u32[]{:S(2)}) async-start(bf16[1,8,256,128]{3,2,0,1:T(8,128)(2,1)} %fusion.29), calls=%async_computation | async-start | bytes 1048576 | tf_op jit(solution)/shard_map/all_to_all | solution.py:129
  76.6 12.3 %all-to-all-start.3 = ((bf16[4,2,256,128]{3,2,1,0:T(8,128)(2,1)}), bf16[4,2,256,128]{3,2,1,0:T(8,128)(2,1)S(1)}, u32[]{:S(2)}, u32[]{:S(2)}) async-start(bf16[4,2,256,128]{3,2,1,0:T(8,128)(2,1)} %bitcast.18), calls=%async_computation.3 | async-start | bytes 1048576 | tf_op jit(solution)/shard_map/all_to_all | solution.py:135
  88.8 13.7 %copy-start.9 = (bf16[1,2,128]{2,1,0:T(2,128)(2,1)S(1)}, bf16[1,2,128]{2,1,0:T(2,128)(2,1)}, u32[]{:S(2)}) copy-start(bf16[1,2,128]{2,1,0:T(2,128)(2,1)} %param.25) | copy-start | bytes 1540
  88.8 12.4 %all-to-all-start.1 = ((bf16[4,2,256,128]{3,2,1,0:T(8,128)(2,1)}), bf16[4,2,256,128]{3,2,1,0:T(8,128)(2,1)S(1)}, u32[]{:S(2)}, u32[]{:S(2)}) async-start(bf16[4,2,256,128]{3,2,1,0:T(8,128)(2,1)} %bitcast.10), calls=%async_computation.1 | async-start | bytes 1048576 | tf_op jit(solution)/shard_map/all_to_all | solution.py:128
  92.7 10.4 %copy-start.1 = (bf16[4,2,256,128]{3,2,0,1:T(8,128)(2,1)}, bf16[4,2,256,128]{3,2,0,1:T(8,128)(2,1)S(1)}, u32[]{:S(2)}) copy-start(bf16[4,2,256,128]{3,2,0,1:T(8,128)(2,1)S(1)} %copy.41) | copy-start | bytes 1572868
  101.3 1.9 %copy-start.2 = (bf16[4,2,256,128]{3,2,0,1:T(8,128)(2,1)}, bf16[4,2,256,128]{3,2,0,1:T(8,128)(2,1)S(1)}, u32[]{:S(2)}) copy-start(bf16[4,2,256,128]{3,2,0,1:T(8,128)(2,1)S(1)} %copy.38) | copy-start | bytes 1572868
